TPU v7x, 128 devices: a whole 4x4x4 slice. The times are simulated.
128 devices in a mesh: rep: 2 (over z_hi), fs: 32 (over z_lo, y, x), tp: 2 (over core).
Axes of the slice: x: 4, y: 4, z: 4 (z_hi: 2, z_lo: 2; z = z_hi * 2 + z_lo), core: 2. Of those that a mesh axis runs over, the one named last changes fastest.
Arguments:
- hidden_in: bfloat16 [40960, 2048], P(('rep', 'fs'), 'tp'), may hold values from -6 to 6
- mix_gain: float32 [2048], replicated, may hold values from 0.1 to 1.9
- w_value: bfloat16 [2048, 1024], P('fs', 'tp'), may hold values from -0.125 to 0.125
- w_gate: bfloat16 [2048, 1024], P('fs', 'tp'), may hold values from -0.125 to 0.125
- conv_taps: float32 [31, 1024], P(None, 'tp'), may hold values from -5 to 5
- conv_bias: float32 [1024], P('tp'), may hold values from -3 to 3
- chan_gain: float32 [1024], P('tp'), may hold values from 0.1 to 1.9
- chan_bias: float32 [1024], P('tp'), may hold values from -3 to 3
- w_back: bfloat16 [1024, 2048], P('tp', 'fs'), may hold values from -0.1875 to 0.1875
- feed_gain: float32 [2048], replicated, may hold values from 0.1 to 1.9
- w_up: bfloat16 [2048, 8192], P(None, ('fs', 'tp')), may hold values from -0.125 to 0.125
- w_down: bfloat16 [8192, 2048], P(('fs', 'tp')), may hold values from -0.0625 to 0.0625
Outputs:
- layer_out: bfloat16 [40960, 2048], P(('rep', 'fs'), 'tp')
All inputs are finite; a program needn't handle non-finite values.
Results may differ from a plain program's by a relative error of at most 0.015.
Values may be sent and summed in bfloat16 or wider, within the bound.
A program may use at most 128 MiB of HBM per device.

v0:
```python
import jax
import jax.numpy as jnp
from jax import lax
from jax.sharding import PartitionSpec as P

KW = 31
LEN = 128


def copy_for_each(array, axis):
    copies = jnp.broadcast_to(array, (lax.axis_size(axis), *array.shape))
    return lax.all_to_all(copies, axis, split_axis=0, concat_axis=0, tiled=True)


def in_order(parts, dim):
    lengths = list(parts.shape[1:])
    lengths[dim] *= parts.shape[0]
    return jnp.moveaxis(parts, 0, dim).reshape(lengths)


def gathered_copies(array, axis, dim):
    parts = copy_for_each(array, axis)
    return in_order(parts, dim)


def side_by_side(arrays, axis, dim, along):
    widths = [a.shape[along] for a in arrays]
    both = jnp.concatenate(arrays, axis=along)
    result = lax.all_gather(both, axis, axis=dim, tiled=True)
    return tuple(jnp.split(result, [sum(widths[:k]) for k in range(1, len(widths))], axis=along))


def in_blocks(array, dim, count):
    lengths = array.shape
    parts = array.reshape(*lengths[:dim], count, lengths[dim] // count, *lengths[dim + 1 :])
    return jnp.moveaxis(parts, dim, 0)


def summed_on_arrival(array, axis, dim):
    count = lax.axis_size(axis)
    parts = lax.all_to_all(in_blocks(array, dim, count), axis, 0, 0, tiled=True)
    return jnp.sum(parts.astype(jnp.float32), axis=0)


def rms_norm(stream, gain):
    values = stream.astype(jnp.float32)
    scaled = values * lax.rsqrt(jnp.mean(values * values, axis=-1, keepdims=True) + 1e-06)
    return (scaled * gain).astype(jnp.bfloat16)


def causal_filter(gated, conv_taps, conv_bias):
    channels = gated.shape[1]
    blocks = gated.reshape(gated.shape[0] // LEN, LEN, channels)
    padded = jnp.pad(blocks, ((0, 0), (KW - 1, 0), (0, 0)))
    result = jnp.zeros_like(blocks) + conv_bias
    for tap_index in range(KW):
        result = result + conv_taps[tap_index] * padded[:, tap_index : tap_index + LEN]
    return result.reshape(gated.shape)


def shards(
    hidden_in,
    mix_gain,
    w_value,
    w_gate,
    conv_taps,
    conv_bias,
    chan_gain,
    chan_bias,
    w_back,
    feed_gain,
    w_up,
    w_down,
):
    gathered = gathered_copies(hidden_in, "tp", 1)
    normed = rms_norm(gathered, mix_gain)
    local_channels = w_value.shape[1]
    whole_value, whole_gate = side_by_side((w_value, w_gate), "fs", 0, 1)
    value_proj = jnp.dot(normed, whole_value, preferred_element_type=jnp.float32)
    gate_proj = jnp.dot(normed, whole_gate, preferred_element_type=jnp.float32)
    gated = value_proj * jax.nn.sigmoid(gate_proj)
    filtered = causal_filter(gated, conv_taps, conv_bias)
    channel_total = local_channels * lax.axis_size("tp")
    first_sum, square_sum = lax.psum(
        (jnp.sum(filtered, axis=1), jnp.sum(filtered * filtered, axis=1)), "tp"
    )
    chan_mean = (first_sum / channel_total)[:, None]
    chan_var = (square_sum / channel_total)[:, None] - chan_mean * chan_mean
    centred = (filtered - chan_mean) * lax.rsqrt(chan_var + 1e-05) * chan_gain + chan_bias
    mixer_act = jax.nn.silu(centred).astype(jnp.bfloat16)
    whole_back = gathered_copies(w_back, "fs", 1)
    partial_value = jnp.dot(mixer_act, whole_back, preferred_element_type=jnp.float32)
    summed = summed_on_arrival(partial_value.astype(jnp.bfloat16), "tp", 1)
    second = (hidden_in.astype(jnp.float32) + summed).astype(jnp.bfloat16)
    gathered_feed = lax.all_gather(second, "tp", axis=1, tiled=True)
    normed_feed = rms_norm(gathered_feed, feed_gain)
    up_proj = jnp.dot(
        normed_feed,
        lax.all_gather(w_up, "fs", axis=1, tiled=True),
        preferred_element_type=jnp.float32,
    )
    hidden = jnp.square(jax.nn.relu(up_proj)).astype(jnp.bfloat16)
    feed_partial = jnp.dot(
        hidden, lax.all_gather(w_down, "fs", axis=0, tiled=True), preferred_element_type=jnp.float32
    )
    feed = summed_on_arrival(feed_partial.astype(jnp.bfloat16), "tp", 1)
    return (second.astype(jnp.float32) + feed).astype(jnp.bfloat16)


def solution(mesh):
    placed = (
        P(("rep", "fs"), "tp"),
        P(),
        P("fs", "tp"),
        P("fs", "tp"),
        P(None, "tp"),
        P("tp"),
        P("tp"),
        P("tp"),
        P("tp", "fs"),
        P(),
        P(None, ("fs", "tp")),
        P(("fs", "tp"), None),
    )
    return jax.shard_map(
        shards, mesh=mesh, in_specs=placed, out_specs=P(("rep", "fs"), "tp"), check_vma=False
    )
```

profile of v0, /device:TPU:1, one launch (start us, length us, event | category | flops | bytes accessed | tf_op | source)
XLA Modules:
  0.0 708.8 jit_solution(11881618682649393780)
XLA Ops:
  6.5 1.5 pad_maximum_fusion
  8.1 1.7 copy.15
  10.0 7.0 all_to_all.20
  17.0 1.6 broadcast_in_dim.5
  18.6 8.6 %all-to-all-start.1 = ((bf16[32,512,64]{1,2,0:T(8,128)(2,1)}), bf16[32,512,64]{1,2,0:T(8,128)(2,1)}, u32[]{:S(2)}, u32[]{:S(2)}) async-start(bf16[32,512,64]{1,2,0:T(8,128)(2,1)} %broadcast_in_dim.5), calls=%async_computation.1 | async-start | bytes 4194304 | tf_op jit(solution)/shard_map/all_to_all | solution.py:12
  27.3 0.6 multiply_reduce_fusion
  28.2 2.2 fusion.4
  30.4 127.4 %all-gather.5.cloned.1.call-done = bf16[2048,1024]{1,0:T(8,128)(2,1)} async-done(((bf16[64,1024]{1,0:T(8,128)(2,1)}), bf16[2048,1024]{1,0:T(8,128)(2,1)}) %all-gather.5.cloned.1.call-update) | async-done | bytes 4194320 | tf_op jit(solution)/shard_map/all_gather | solution.py:29
  157.8 4.2 fusion.28
  162.1 1.6 fusion.16
  163.7 5.5 fusion.93
  169.2 22.1 %all-reduce.1 = (f32[640]{0:T(1024)S(1)}, f32[640]{0:T(1024)S(1)}) all-reduce(f32[640]{0:T(1024)S(1)} %bitcast.77, f32[640]{0:T(1024)S(1)} %bitcast.76), channel_id=1, replica_groups=mesh['rep'=2,'fs'=32,'tp'=2] {'tp'}, use_global_device_ids=true, to_apply=%region_4.5 | all-reduce | flops 1280 | bytes 10240 | tf_op jit(solution)/shard_map/psum | solution.py:84
  191.2 0.5 multiply_convert_fusion.1
  191.8 3.1 convolution_convert_fusion
  194.9 0.3 copy.23
  195.2 5.8 all_to_all.21
  201.0 0.6 convert_reduce_fusion.1
  201.6 0.7 copy-done.2
  202.3 1.5 add_convert_fusion.1
  204.0 0.7 all-gather.11.cloned.1.call-update
  204.6 0.2 all-gather.9.cloned.1.call-start
  204.9 0.3 all-gather.9.cloned.1.call-update
  205.2 13.4 %all-gather.7.cloned.1.call-done = bf16[640,2048]{1,0:T(8,128)(2,1)} async-done(((bf16[640,1024]{1,0:T(8,128)(2,1)}), bf16[640,2048]{1,0:T(8,128)(2,1)}) %all-gather.7.cloned.1.call-update) | async-done | bytes 2621456 | tf_op jit(solution)/shard_map/all_gather | solution.py:95
  218.7 2.5 fusion
  221.2 190.3 %all-gather.11.cloned.1.call-done = bf16[4096,2048]{1,0:T(8,128)(2,1)} async-done(((bf16[128,2048]{1,0:T(8,128)(2,1)}), bf16[4096,2048]{1,0:T(8,128)(2,1)}) %all-gather.11.cloned.1.call-update) | async-done | bytes 16777232 | tf_op jit(solution)/shard_map/all_gather | solution.py:104
  411.5 222.9 %all-gather.9.cloned.1.call-done = bf16[2048,4096]{1,0:T(8,128)(2,1)} async-done(((bf16[2048,128]{1,0:T(8,128)(2,1)}), bf16[2048,4096]{1,0:T(8,128)(2,1)}) %all-gather.9.cloned.1.call-update) | async-done | bytes 16777232 | tf_op jit(solution)/shard_map/all_gather | solution.py:99
  634.4 33.8 %convolution_convert_fusion.1 = bf16[640,2048]{1,0:T(8,128)(2,1)} fusion(bf16[4096,2048]{1,0:T(8,128)(2,1)} %all-gather.11.cloned.1.call-done, bf16[2048,4096]{1,0:T(8,128)(2,1)} %all-gather.9.cloned.1.call-done, bf16[640,2048]{1,0:T(8,128)(2,1)S(1)} %copy-done.3, f32[2048]{0:T(1024)S(1)} %copy-done.11, f32[640]{0:T(1024)S(1)} %add_rsqrt_fusion), kind=kOutput, calls=%fused_computation.43 | convolution fusion | flops 21489254400 | bytes 38808064 | tf_op jit(solution)/shard_map/dot_general | solution.py:103
  668.2 2.0 copy.22
  670.2 29.3 %all_to_all.22 = bf16[2,640,1024]{2,1,0:T(8,128)(2,1)S(1)} all-to-all(bf16[2,640,1024]{2,1,0:T(8,128)(2,1)S(1)} %bitcast.71), channel_id=1, replica_groups=mesh['rep'=2,'fs'=32,'tp'=2] {'tp'}, dimensions={0} | all-to-all | bytes 5242880 | tf_op jit(solution)/shard_map/all_to_all | solution.py:41
  699.4 0.6 convert_reduce_fusion
  700.0 0.7 copy-done
  700.8 1.5 add_convert_fusion
  (34 shorter events, 0.6 us)
Async XLA Ops:
  6.5 151.2 %all-gather.5.cloned.1.call-start = ((), (), s32[]{:S(2)}) async-start(), calls=%async_computation.4 | async-start | bytes 4325376 | tf_op jit(solution)/shard_map/all_gather | solution.py:29
  10.0 7.0 copy-start.5
  18.6 173.2 %all-to-all-start.1 = ((bf16[32,512,64]{1,2,0:T(8,128)(2,1)}), bf16[32,512,64]{1,2,0:T(8,128)(2,1)}, u32[]{:S(2)}, u32[]{:S(2)}) async-start(bf16[32,512,64]{1,2,0:T(8,128)(2,1)} %broadcast_in_dim.5), calls=%async_computation.1 | async-start | bytes 4194304 | tf_op jit(solution)/shard_map/all_to_all | solution.py:12
  27.3 0.8 copy-start.6
  27.3 0.9 copy-start.7
  27.3 191.4 %all-gather.7.cloned.1.call-start = ((), (), s32[]{:S(2)}) async-start(), calls=%async_computation.5 | async-start | bytes 3932160 | tf_op jit(solution)/shard_map/all_gather | solution.py:95
  30.4 131.7 %copy-start.1 = (bf16[640,2048]{0,1:T(8,128)(2,1)S(1)}, bf16[640,2048]{0,1:T(8,128)(2,1)}, u32[]{:S(2)}) copy-start(bf16[640,2048]{0,1:T(8,128)(2,1)} %fusion.4) | copy-start | bytes 7864324
  157.8 4.3 copy-start.4
  162.0 1.6 copy-start.8
  163.7 27.6 %copy-start.9 = (f32[512]{0:T(512)S(1)}, f32[512]{0:T(512)}, u32[]{:S(2)}) copy-start(f32[512]{0:T(512)} %param.19) | copy-start | bytes 6148
  163.7 27.6 %copy-start.10 = (f32[512]{0:T(512)S(1)}, f32[512]{0:T(512)}, u32[]{:S(2)}) copy-start(f32[512]{0:T(512)} %param.18) | copy-start | bytes 6148
  201.0 1.3 copy-start.2
  203.9 207.6 %all-gather.11.cloned.1.call-start = ((), (), s32[]{:S(2)}) async-start(), calls=%async_computation.7 | async-start | bytes 17301504 | tf_op jit(solution)/shard_map/all_gather | solution.py:104
  204.6 429.8 %all-gather.9.cloned.1.call-start = ((), (), s32[]{:S(2)}) async-start(), calls=%async_computation.6 | async-start | bytes 17301504 | tf_op jit(solution)/shard_map/all_gather | solution.py:99
  205.2 429.2 %copy-start.11 = (f32[2048]{0:T(1024)S(1)}, f32[2048]{0:T(1024)}, u32[]{:S(2)}) copy-start(f32[2048]{0:T(1024)} %param.21) | copy-start | bytes 24580
  218.7 415.7 %copy-start.3 = (bf16[640,2048]{1,0:T(8,128)(2,1)S(1)}, bf16[640,2048]{1,0:T(8,128)(2,1)}, u32[]{:S(2)}) copy-start(bf16[640,2048]{1,0:T(8,128)(2,1)} %all-gather.7.cloned.1.call-done) | copy-start | bytes 7864324
  699.4 1.3 copy-start
Sparse Core Ops, SparseCore 0:
  9.0 148.7 all-gather.4
  204.0 14.6 all-gather.6
  220.3 191.0 all-gather.10
  412.9 221.4 all-gather.8
where the time goes:
time: 709 us
  waiting for transfers between devices  555 us (78%)
  blocking collectives  64.1 us (9%)
  matrix products  42.7 us (6%)
  other arithmetic  17 us (2%)
  between operations  13.3 us (2%)
  starting transfers between devices  8.94 us (1%)
  local copies, waits for them, and re-layouts  7.52 us (1%)
    all_gather x1, waiting for transfers between devices, shards(): lax.all_gather(w_up, 'fs', axis=1, tiled=True)  223 us
    all_gather x1, waiting for transfers between devices, shards(): lax.all_gather(w_down, 'fs', axis=0, tiled=True)  190 us
    all_gather x1, waiting for transfers between devices, side_by_side(): result = lax.all_gather(both, axis, axis=dim, tiled=True)  127 us
    all_to_all x2, blocking collectives, summed_on_arrival(): parts = lax.all_to_all(in_blocks(array, dim, count), axis, 0, 0, tiled=True)  35.1 us
    dot_general x1, matrix products, shards(): jnp.dot(hidden, lax.all_gather(w_down, 'fs', axis=0, tiled=True), preferr...  33.8 us
    psum x1, blocking collectives, shards(): lax.psum((jnp.sum(filtered, axis=1), jnp.sum(filtered * filtered, axis=1)...  22.1 us
  transfers between devices with their start and end apart: 5, of which 4 were waited for; matrix products, arithmetic and copies ran while one was open for 3% of the time, Pallas kernels for 0%

commit v1 on v0

--- a/solution.py
+++ b/solution.py
@@ -101,7 +101,11 @@
     )
     hidden = jnp.square(jax.nn.relu(up_proj)).astype(jnp.bfloat16)
     feed_partial = jnp.dot(
-        hidden, lax.all_gather(w_down, "fs", axis=0, tiled=True), preferred_element_type=jnp.float32
+        hidden,
+        jnp.concatenate(
+            lax.all_to_all(jnp.stack([w_down] * lax.axis_size("fs")), "fs", 0, 0), axis=0
+        ),
+        preferred_element_type=jnp.float32,
     )
     feed = summed_on_arrival(feed_partial.astype(jnp.bfloat16), "tp", 1)
     return (second.astype(jnp.float32) + feed).astype(jnp.bfloat16)

time: 709 us -> 723 us (1.020)
  blocking collectives: 64.1 us -> 50.8 us
  waiting for transfers between devices: 555 us -> 568 us
    all_to_all x0 -> x1, waiting for transfers between devices: none -> 300 us  [shards(): lax.all_to_all(jnp.stack([w_down] * lax.axis_size('fs')), 'fs', 0, 0)]
    all_gather x1 -> x0, waiting for transfers between devices: 190 us -> none  [shards(): lax.all_gather(w_down, 'fs', axis=0, tiled=True)]
    all_gather x1, waiting for transfers between devices: 223 us -> 139 us  [shards(): lax.all_gather(w_up, 'fs', axis=1, tiled=True)]
    all_to_all x2, blocking collectives: 35.1 us -> 21.7 us  [summed_on_arrival(): parts = lax.all_to_all(in_blocks(array, dim, count), axis, 0, 0, tiled=True)]
    all_gather x1, waiting for transfers between devices: 13.4 us -> 0.84 us  [shards(): gathered_feed = lax.all_gather(second, 'tp', axis=1, tiled=True)]
  transfers between devices with their start and end apart: 5 -> 5, of which waited for: 4 -> 4; matrix products, arithmetic and copies ran while one was open for 3% -> 4% of each run, Pallas kernels for 0% -> 0%
where the time goes in v1:
time: 723 us; the launch traced here: 721 us
  waiting for transfers between devices  568 us (79%)
  blocking collectives  50.8 us (7%)
  matrix products  42.7 us (6%)
  other arithmetic  17 us (2%)
  starting transfers between devices  15.7 us (2%)
  local copies, waits for them, and re-layouts  13.7 us (2%)
  between operations  13.3 us (2%)
    all_to_all x1, waiting for transfers between devices, shards(): lax.all_to_all(jnp.stack([w_down] * lax.axis_size('fs')), 'fs', 0, 0)  300 us
    all_gather x1, waiting for transfers between devices, shards(): lax.all_gather(w_up, 'fs', axis=1, tiled=True)  139 us
    all_gather x1, waiting for transfers between devices, side_by_side(): result = lax.all_gather(both, axis, axis=dim, tiled=True)  127 us
    dot_general x1, matrix products, shards(): jnp.dot(hidden, jnp.concatenate(lax.all_to_all(jnp.stack([w_down] * lax.a...  33.8 us
    psum x1, blocking collectives, shards(): lax.psum((jnp.sum(filtered, axis=1), jnp.sum(filtered * filtered, axis=1)...  22.1 us
    all_to_all x2, blocking collectives, summed_on_arrival(): parts = lax.all_to_all(in_blocks(array, dim, count), axis, 0, 0, tiled=True)  21.7 us
  transfers between devices with their start and end apart: 5, of which 4 were waited for; matrix products, arithmetic and copies ran while one was open for 4% of the time, Pallas kernels for 0%

profile of v1, /device:TPU:1, one launch (start us, length us, event | category | flops | bytes accessed | tf_op | source)
XLA Modules:
  0.0 721.4 jit_solution(12222752151592111392)
XLA Ops:
  6.5 1.5 pad_maximum_fusion
  8.1 1.7 copy.15
  10.0 7.0 all_to_all.25
  17.0 1.6 broadcast_in_dim.5
  18.6 8.6 %all-to-all-start.1 = ((bf16[32,512,64]{1,2,0:T(8,128)(2,1)}), bf16[32,512,64]{1,2,0:T(8,128)(2,1)}, u32[]{:S(2)}, u32[]{:S(2)}) async-start(bf16[32,512,64]{1,2,0:T(8,128)(2,1)} %broadcast_in_dim.5), calls=%async_computation.1 | async-start | bytes 4194304 | tf_op jit(solution)/shard_map/all_to_all | solution.py:12
  27.3 0.6 multiply_reduce_fusion
  28.2 2.2 fusion.4
  30.4 127.4 %all-gather.4.cloned.1.call-done = bf16[2048,1024]{1,0:T(8,128)(2,1)} async-done(((bf16[64,1024]{1,0:T(8,128)(2,1)}), bf16[2048,1024]{1,0:T(8,128)(2,1)}) %all-gather.4.cloned.1.call-update) | async-done | bytes 4194320 | tf_op jit(solution)/shard_map/all_gather | solution.py:29
  157.8 4.2 fusion.28
  162.1 1.6 fusion.16
  163.7 5.5 fusion.93
  169.2 22.1 %all-reduce.1 = (f32[640]{0:T(1024)S(1)}, f32[640]{0:T(1024)S(1)}) all-reduce(f32[640]{0:T(1024)S(1)} %bitcast.78, f32[640]{0:T(1024)S(1)} %bitcast.77), channel_id=1, replica_groups=mesh['rep'=2,'fs'=32,'tp'=2] {'tp'}, use_global_device_ids=true, to_apply=%region_4.5 | all-reduce | flops 1280 | bytes 10240 | tf_op jit(solution)/shard_map/psum | solution.py:84
  191.2 0.5 multiply_convert_fusion.1
  191.8 3.1 convolution_convert_fusion
  194.9 0.3 copy.23
  195.2 5.8 all_to_all.26
  201.0 0.6 convert_reduce_fusion.1
  201.6 0.7 copy-done.2
  202.3 1.5 add_convert_fusion.1
  204.0 0.7 all-gather.8.cloned.1.call-update
  204.9 5.9 stack.2
  210.9 7.0 all-to-all-start.3
  217.8 0.8 all-gather.6.cloned.1.call-done
  218.7 2.5 fusion
  221.2 300.2 %all-to-all-done.3 = bf16[32,128,2048]{2,1,0:T(8,128)(2,1)} async-done(((bf16[32,128,2048]{2,1,0:T(8,128)(2,1)}), bf16[32,128,2048]{2,1,0:T(8,128)(2,1)}, u32[]{:S(2)}, u32[]{:S(2)}) %all-to-all-start.3) | async-done | bytes 16777248 | tf_op jit(solution)/shard_map/all_to_all | solution.py:106
  521.4 139.0 %all-gather.8.cloned.1.call-done = bf16[2048,4096]{1,0:T(8,128)(2,1)} async-done(((bf16[2048,128]{1,0:T(8,128)(2,1)}), bf16[2048,4096]{1,0:T(8,128)(2,1)}) %all-gather.8.cloned.1.call-update) | async-done | bytes 16777232 | tf_op jit(solution)/shard_map/all_gather | solution.py:99
  660.4 33.8 %convolution_convert_fusion.1 = bf16[640,2048]{1,0:T(8,128)(2,1)} fusion(bf16[4096,2048]{1,0:T(8,128)(2,1)} %bitcast.42, bf16[2048,4096]{1,0:T(8,128)(2,1)} %all-gather.8.cloned.1.call-done, bf16[640,2048]{1,0:T(8,128)(2,1)S(1)} %copy-done.3, f32[2048]{0:T(1024)S(1)} %copy-done.12, f32[640]{0:T(1024)S(1)} %add_rsqrt_fusion), kind=kOutput, calls=%fused_computation.43 | convolution fusion | flops 21489254400 | bytes 38808064 | tf_op jit(solution)/shard_map/dot_general | solution.py:103
  694.1 2.0 copy.22
  696.1 15.9 %all_to_all.27 = bf16[2,640,1024]{2,1,0:T(8,128)(2,1)S(1)} all-to-all(bf16[2,640,1024]{2,1,0:T(8,128)(2,1)S(1)} %bitcast.72), channel_id=1, replica_groups=mesh['rep'=2,'fs'=32,'tp'=2] {'tp'}, dimensions={0} | all-to-all | bytes 5242880 | tf_op jit(solution)/shard_map/all_to_all | solution.py:41
  712.0 0.6 convert_reduce_fusion
  712.6 0.7 copy-done
  713.4 1.5 add_convert_fusion
  (36 shorter events, 0.9 us)
Async XLA Ops:
  6.5 151.2 %all-gather.4.cloned.1.call-start = ((), (), s32[]{:S(2)}) async-start(), calls=%async_computation.5 | async-start | bytes 4325376 | tf_op jit(solution)/shard_map/all_gather | solution.py:29
  10.0 7.0 copy-start.6
  18.6 173.2 %all-to-all-start.1 = ((bf16[32,512,64]{1,2,0:T(8,128)(2,1)}), bf16[32,512,64]{1,2,0:T(8,128)(2,1)}, u32[]{:S(2)}, u32[]{:S(2)}) async-start(bf16[32,512,64]{1,2,0:T(8,128)(2,1)} %broadcast_in_dim.5), calls=%async_computation.1 | async-start | bytes 4194304 | tf_op jit(solution)/shard_map/all_to_all | solution.py:12
  27.3 0.8 copy-start.7
  27.3 0.9 copy-start.8
  27.3 191.4 %all-gather.6.cloned.1.call-start = ((), (), s32[]{:S(2)}) async-start(), calls=%async_computation.6 | async-start | bytes 3932160 | tf_op jit(solution)/shard_map/all_gather | solution.py:95
  30.4 131.7 %copy-start.1 = (bf16[640,2048]{0,1:T(8,128)(2,1)S(1)}, bf16[640,2048]{0,1:T(8,128)(2,1)}, u32[]{:S(2)}) copy-start(bf16[640,2048]{0,1:T(8,128)(2,1)} %fusion.4) | copy-start | bytes 7864324
  157.8 4.3 copy-start.4
  162.0 1.6 copy-start.9
  163.7 27.6 %copy-start.10 = (f32[512]{0:T(512)S(1)}, f32[512]{0:T(512)}, u32[]{:S(2)}) copy-start(f32[512]{0:T(512)} %param.19) | copy-start | bytes 6148
  163.7 27.6 %copy-start.11 = (f32[512]{0:T(512)S(1)}, f32[512]{0:T(512)}, u32[]{:S(2)}) copy-start(f32[512]{0:T(512)} %param.18) | copy-start | bytes 6148
  201.0 1.3 copy-start.2
  203.9 1.0 copy-start.5
  203.9 456.4 %all-gather.8.cloned.1.call-start = ((), (), s32[]{:S(2)}) async-start(), calls=%async_computation.7 | async-start | bytes 17301504 | tf_op jit(solution)/shard_map/all_gather | solution.py:99
  210.9 310.5 %all-to-all-start.3 = ((bf16[32,128,2048]{2,1,0:T(8,128)(2,1)}), bf16[32,128,2048]{2,1,0:T(8,128)(2,1)}, u32[]{:S(2)}, u32[]{:S(2)}) async-start(bf16[32,128,2048]{2,1,0:T(8,128)(2,1)} %stack.2), calls=%async_computation.3 | async-start | bytes 33554432 | tf_op jit(solution)/shard_map/all_to_all | solution.py:106
  217.8 442.5 %copy-start.12 = (f32[2048]{0:T(1024)S(1)}, f32[2048]{0:T(1024)}, u32[]{:S(2)}) copy-start(f32[2048]{0:T(1024)} %param.21) | copy-start | bytes 24580
  218.7 441.7 %copy-start.3 = (bf16[640,2048]{1,0:T(8,128)(2,1)S(1)}, bf16[640,2048]{1,0:T(8,128)(2,1)}, u32[]{:S(2)}) copy-start(bf16[640,2048]{1,0:T(8,128)(2,1)} %all-gather.6.cloned.1.call-done) | copy-start | bytes 7864324
  712.0 1.3 copy-start
Sparse Core Ops, SparseCore 0:
  9.0 148.7 all-gather.3
  204.0 14.6 all-gather.5
  220.3 440.0 all-gather.7
